TPU v7x, 32 devices: a whole 2x2x4 slice. The times are simulated.
32 devices in a mesh: kv: 8 (over z, x), tp: 4 (over y, core).
Axes of the slice: x: 2, y: 2, z: 4, core: 2. Of those that a mesh axis runs over, the one named last changes fastest.
Arguments:
- tokens: bfloat16 [22, 4096], P(None, ('kv', 'tp')), may hold values from -22 to 22
- attn_gain: float32 [4096], P('kv'), may hold values from 0.1 to 1.9
- w_query: bfloat16 [4096, 4096], P('kv', 'tp'), may hold values from -0.09375 to 0.09375
- w_key: bfloat16 [4096, 4096], P('kv', 'tp'), may hold values from -0.5 to 0.5
- w_value: bfloat16 [4096, 4096], P('kv', 'tp'), may hold values from -0.09375 to 0.09375
- cache_keys: bfloat16 [22, 2048, 32, 128], P(None, 'kv', 'tp'), may hold values from -256 to 256
- cache_values: bfloat16 [22, 2048, 32, 128], P(None, 'kv', 'tp'), may hold values from -6 to 6
- lambdas: float32 [32], P('tp'), may hold values from 0.3 to 0.8
- head_gain: float32 [128], replicated, may hold values from 0.1 to 1.9
- w_out: bfloat16 [4096, 4096], P('tp', 'kv'), may hold values from -0.09375 to 0.09375
- mlp_gain: float32 [4096], P('kv'), may hold values from 0.1 to 1.9
- w_gate: bfloat16 [4096, 11008], P('kv', 'tp'), may hold values from -0.09375 to 0.09375
- w_up: bfloat16 [4096, 11008], P('kv', 'tp'), may hold values from -0.09375 to 0.09375
- w_down: bfloat16 [11008, 4096], P('tp', 'kv'), may hold values from -0.0546875 to 0.0546875
Outputs:
- output: bfloat16 [22, 4096], P(None, ('kv', 'tp'))
All inputs are finite; a program needn't handle non-finite values.
Results may differ from a plain program's by a relative error of at most 0.017.
The roundings to bfloat16 on the way count: a program that leaves them out, or rounds other values in their place, can miss the bound.
Values may be sent and summed in bfloat16 or wider, within the bound.
A program may use at most 128 MiB of HBM per device.

v0:
```python
import jax
import jax.numpy as jnp
from jax import lax
from jax.sharding import PartitionSpec as P

D = 4096
epsilon = 1e-06


def combined_all(value, axis, join):
    pieces = jax.tree.map(lambda part: lax.all_gather(part, axis), value)
    head = jax.tree.map(lambda part: part[0], pieces)
    tail = jax.tree.map(lambda part: part[1:], pieces)
    running, _ = lax.scan(lambda running, section: (join(running, section), None), head, tail)
    return running


def join_map(left_max, left_sum, left_val, right_max, right_sum, right_val):
    peak_val = jnp.maximum(left_max, right_max)
    left_weight = jnp.exp(left_max - peak_val)
    right_weight = jnp.exp(right_max - peak_val)
    return (
        peak_val,
        left_sum * left_weight + right_sum * right_weight,
        left_val * left_weight[..., None] + right_val * right_weight[..., None],
    )


def combine(earlier, later):
    return join_map(earlier[0], earlier[1], earlier[2], later[0], later[1], later[2]) + join_map(
        earlier[3], earlier[4], earlier[5], later[3], later[4], later[5]
    )


def per_device(
    tokens,
    attn_gain,
    w_query,
    w_key,
    w_value,
    cache_keys,
    cache_values,
    lambdas,
    head_gain,
    w_out,
    mlp_gain,
    w_gate,
    w_up,
    w_down,
):
    seq_count = tokens.shape[0]
    own_width = tokens.shape[1]
    local_heads = lambdas.shape[0]
    head_dim = head_gain.shape[0]
    half_dim = head_dim // 2
    score_scale = half_dim ** (-0.5)
    gathered = lax.all_gather(tokens, "tp", axis=1, tiled=True)
    gathered_f = gathered.astype(jnp.float32)
    normed_in = (gathered_f * attn_gain).astype(jnp.bfloat16)
    query_part = jnp.dot(normed_in, w_query, preferred_element_type=jnp.float32)
    key_part = jnp.dot(normed_in, w_key, preferred_element_type=jnp.float32)
    value_part = jnp.dot(normed_in, w_value, preferred_element_type=jnp.float32)
    query_sum, key_sum, value_sum, square_sum = lax.psum(
        (query_part, key_part, value_part, jnp.sum(gathered_f * gathered_f, axis=1, keepdims=True)),
        "kv",
    )
    scale_in = lax.rsqrt(square_sum / D + epsilon)
    query_rows = (
        (scale_in * query_sum).astype(jnp.bfloat16).reshape(seq_count, local_heads, head_dim)
    )
    key_new = (scale_in * key_sum).astype(jnp.bfloat16).reshape(seq_count, local_heads, head_dim)
    value_new = (
        (scale_in * value_sum).astype(jnp.bfloat16).reshape(seq_count, local_heads, head_dim)
    )

    def partial_map(low, high):
        scores = (
            jnp.einsum(
                "shd,sthd->sht",
                query_rows[:, :, low:high],
                cache_keys[:, :, :, low:high],
                preferred_element_type=jnp.float32,
            )
            * score_scale
        )
        maxima = jnp.max(scores, axis=2)
        weights = jnp.exp(scores - maxima[:, :, None])
        totals = jnp.sum(weights, axis=2)
        summed = jnp.einsum(
            "sht,sthd->shd",
            weights.astype(jnp.bfloat16),
            cache_values,
            preferred_element_type=jnp.float32,
        )
        return (maxima, totals, summed)

    def own_term(low, high):
        score_new = (
            jnp.sum(
                query_rows[:, :, low:high].astype(jnp.float32)
                * key_new[:, :, low:high].astype(jnp.float32),
                axis=2,
            )
            * score_scale
        )
        return (score_new, jnp.ones_like(score_new), value_new.astype(jnp.float32))

    first_part = partial_map(0, half_dim)
    second_part = partial_map(half_dim, head_dim)
    merged = combined_all(
        (
            first_part[0],
            first_part[1],
            first_part[2],
            second_part[0],
            second_part[1],
            second_part[2],
        ),
        "kv",
        combine,
    )
    combined = combine(merged, own_term(0, half_dim) + own_term(half_dim, head_dim))
    first_map = combined[2] / combined[1][:, :, None]
    second_map = combined[5] / combined[4][:, :, None]
    difference = first_map - lambdas[None, :, None] * second_map
    normed = (
        difference
        * lax.rsqrt(jnp.mean(difference * difference, axis=2, keepdims=True) + epsilon)
        * head_gain
    )
    heads_out = normed.astype(jnp.bfloat16).reshape(seq_count, local_heads * head_dim)
    branch = lax.psum(
        jnp.dot(heads_out, w_out, preferred_element_type=jnp.float32).astype(jnp.bfloat16), "tp"
    ).astype(jnp.float32)
    residual = (gathered_f + branch).astype(jnp.bfloat16)
    residual_f = residual.astype(jnp.float32)
    mid_sum = lax.psum(jnp.sum(residual_f * residual_f, axis=1, keepdims=True), "kv")
    scale_mid = lax.rsqrt(mid_sum / D + epsilon)
    normed_mid = (residual_f * mlp_gain).astype(jnp.bfloat16)
    gate_part = jnp.dot(normed_mid, w_gate, preferred_element_type=jnp.float32)
    up_part = jnp.dot(normed_mid, w_up, preferred_element_type=jnp.float32)
    gate_sum, up_sum = lax.psum((gate_part, up_part), "kv")
    hidden = (jax.nn.silu(scale_mid * gate_sum) * (scale_mid * up_sum)).astype(jnp.bfloat16)
    down_part = jnp.dot(hidden, w_down, preferred_element_type=jnp.float32).astype(jnp.bfloat16)
    mixer_own = lax.psum_scatter(down_part, "tp", scatter_dimension=1, tiled=True).astype(
        jnp.float32
    )
    tp_index = lax.axis_index("tp")
    residual_own = lax.dynamic_slice_in_dim(residual_f, tp_index * own_width, own_width, 1)
    return (residual_own + mixer_own).astype(jnp.bfloat16)


def solution(mesh):
    in_specs = (
        P(None, ("kv", "tp")),
        P("kv"),
        P("kv", "tp"),
        P("kv", "tp"),
        P("kv", "tp"),
        P(None, "kv", "tp", None),
        P(None, "kv", "tp", None),
        P("tp"),
        P(),
        P("tp", "kv"),
        P("kv"),
        P("kv", "tp"),
        P("kv", "tp"),
        P("tp", "kv"),
    )
    out_specs = P(None, ("kv", "tp"))
    return jax.shard_map(
        per_device, mesh=mesh, in_specs=in_specs, out_specs=out_specs, check_vma=False
    )
```

profile of v0, /device:TPU:0, one launch (start us, length us, event | category | flops | bytes accessed | tf_op | source)
XLA Modules:
  0.0 441.2 jit_solution(7946327300778123110)
XLA Ops:
  6.5 6.5 %all_gather.39 = bf16[22,512]{1,0:T(8,128)(2,1)S(1)} all-gather(bf16[22,128]{1,0:T(8,128)(2,1)} %param.16), channel_id=1, replica_groups=mesh['kv'=8,'tp'=4] {'tp'}, dimensions={1}, use_global_device_ids=true | all-gather | bytes 28160 | tf_op jit(solution)/shard_map/all_gather | solution.py:57
  13.0 2.1 fusion.35
  15.2 2.1 fusion.33
  17.3 2.1 fusion.37
  19.5 17.3 %fusion.54 = (bf16[22,256,8,64]{3,2,1,0:T(8,128)(2,1)}, bf16[22,256,8,64]{3,2,1,0:T(8,128)(2,1)}) fusion(bf16[22,256,8,128]{3,2,1,0:T(8,128)(2,1)} %param.21), kind=kLoop, calls=%fused_computation.89 | loop fusion | bytes 23068672 | tf_op jit(solution)/shard_map/slice | solution.py:81
  36.8 0.1 fusion.28
  36.9 22.2 %psum.56 = f32[22,1]{0,1:T(1,128)S(1)} all-reduce(f32[22,1]{0,1:T(1,128)S(1)} %bitcast.129), channel_id=1, replica_groups=mesh['kv'=8,'tp'=4] {'kv'}, use_global_device_ids=true, to_apply=%region_1.0 | all-reduce | flops 22 | bytes 176 | tf_op jit(solution)/shard_map/psum | solution.py:63
  59.1 34.2 %all-reduce.7.cloned.1.call-done = (f32[22,1024]{1,0:T(8,128)}, f32[22,1024]{1,0:T(8,128)}, f32[22,1024]{1,0:T(8,128)}) async-done(((f32[22,1024]{1,0:T(8,128)}, f32[22,1024]{1,0:T(8,128)}, f32[22,1024]{1,0:T(8,128)}), (f32[22,1024]{1,0:T(8,128)}, f32[22,1024]{1,0:T(8,128)}, f32[22,1024]{1,0:T(8,128)})) %all-reduce.7.cloned.1.call-update) | async-done | bytes 270352 | tf_op jit(solution)/shard_map/psum | solution.py:63
  93.3 1.1 fusion.31
  94.5 7.4 %fusion.6 = f32[22,8,1,256]{3,2,1,0:T(1,128)S(1)} fusion(bf16[22,256,8,64]{3,2,1,0:T(8,128)(2,1)} %get-tuple-element.134, bf16[22,8,64,1]{2,1,0,3:T(8,128)(2,1)S(1)} %get-tuple-element.142), kind=kOutput, calls=%fused_computation.16 | convolution fusion | flops 5767168 | bytes 5969920 | tf_op jit(solution)/shard_map/shd,sthd->sht/dot_general | solution.py:78
  101.8 0.1 fusion.21
  101.9 0.2 fusion.24
  102.2 30.6 %all-gather.8 = f32[8,22,8]{1,2,0:T(8,128)S(1)} all-gather(f32[1,22,8]{1,2,0:T(8,128)S(1)} %copy.59), channel_id=5, replica_groups=mesh['kv'=8,'tp'=4] {'kv'}, dimensions={0}, use_global_device_ids=true | all-gather | bytes 6336 | tf_op jit(solution)/shard_map/all_gather | solution.py:11
  132.9 30.6 %all-gather.9 = f32[8,22,8]{1,2,0:T(8,128)S(1)} all-gather(f32[1,22,8]{1,2,0:T(8,128)S(1)} %copy.60), channel_id=6, replica_groups=mesh['kv'=8,'tp'=4] {'kv'}, dimensions={0}, use_global_device_ids=true | all-gather | bytes 6336 | tf_op jit(solution)/shard_map/all_gather | solution.py:11
  163.5 7.4 %fusion.8 = f32[22,8,1,256]{3,2,1,0:T(1,128)S(1)} fusion(bf16[22,256,8,64]{3,2,1,0:T(8,128)(2,1)} %get-tuple-element.135, bf16[22,8,64,1]{2,1,0,3:T(8,128)(2,1)S(1)} %get-tuple-element.143), kind=kOutput, calls=%fused_computation.18 | convolution fusion | flops 5767168 | bytes 5969920 | tf_op jit(solution)/shard_map/shd,sthd->sht/dot_general | solution.py:78
  170.8 0.1 fusion.20
  171.0 0.2 fusion.25
  171.2 30.6 %all-gather.6 = f32[8,22,8]{1,2,0:T(8,128)S(1)} all-gather(f32[1,22,8]{1,2,0:T(8,128)S(1)} %copy.57), channel_id=2, replica_groups=mesh['kv'=8,'tp'=4] {'kv'}, dimensions={0}, use_global_device_ids=true | all-gather | bytes 6336 | tf_op jit(solution)/shard_map/all_gather | solution.py:11
  201.9 30.6 %all-gather.7 = f32[8,22,8]{1,2,0:T(8,128)S(1)} all-gather(f32[1,22,8]{1,2,0:T(8,128)S(1)} %copy.58), channel_id=3, replica_groups=mesh['kv'=8,'tp'=4] {'kv'}, dimensions={0}, use_global_device_ids=true | all-gather | bytes 6336 | tf_op jit(solution)/shard_map/all_gather | solution.py:11
  232.5 5.9 %fusion.12 = f32[22,8,1,128]{3,2,1,0:T(1,128)S(1)} fusion(bf16[22,256,8,128]{3,2,1,0:T(8,128)(2,1)} %param.22, bf16[22,8,256,1]{2,1,0,3:T(8,128)(2,1)S(1)} %get-tuple-element.138), kind=kOutput, calls=%fused_computation.22 | convolution fusion | flops 11534336 | bytes 11714560 | tf_op jit(solution)/shard_map/sht,sthd->shd/dot_general | solution.py:89
  238.5 32.1 %all-gather.2 = f32[176,8,128]{2,1,0:T(8,128)S(1)} all-gather(f32[22,8,128]{2,1,0:T(8,128)S(1)} %bitcast.123), channel_id=4, replica_groups=mesh['kv'=8,'tp'=4] {'kv'}, dimensions={0}, use_global_device_ids=true | all-gather | bytes 811008 | tf_op jit(solution)/shard_map/all_gather | solution.py:11
  270.5 0.9 slice.104
  271.4 5.9 %fusion.10 = f32[22,8,1,128]{3,2,1,0:T(1,128)S(1)} fusion(bf16[22,256,8,128]{3,2,1,0:T(8,128)(2,1)} %param.22, bf16[22,8,256,1]{2,1,0,3:T(8,128)(2,1)S(1)} %get-tuple-element.136), kind=kOutput, calls=%fused_computation.20 | convolution fusion | flops 11534336 | bytes 11714560 | tf_op jit(solution)/shard_map/sht,sthd->shd/dot_general | solution.py:89
  277.3 31.7 %all-gather.5 = f32[176,8,128]{2,1,0:T(8,128)S(1)} all-gather(f32[22,8,128]{2,1,0:T(8,128)S(1)} %bitcast.124), channel_id=7, replica_groups=mesh['kv'=8,'tp'=4] {'kv'}, dimensions={0}, use_global_device_ids=true | all-gather | bytes 811008 | tf_op jit(solution)/shard_map/all_gather | solution.py:11
  309.0 0.9 slice.107
  309.9 0.2 multiply_reduce_fusion.2
  310.2 10.7 %while.20 = (s32[]{:T(128)}, f32[22,8]{0,1:T(8,128)S(1)}, f32[22,8]{0,1:T(8,128)S(1)}, f32[22,8,128]{2,1,0:T(8,128)S(1)}, f32[22,8]{0,1:T(8,128)S(1)}, /*index=5...) while((s32[]{:T(128)}, f32[22,8]{0,1:T(8,128)S(1)}, ...), condition=%wide.region_8.0_spmd, body=%wide.region_7.0_spmd.sunk | while | flops 137282 | bytes 560537 | solution.py:14
  310.6 1.1 fusion.68
  312.1 1.1 fusion.68
  313.7 1.1 fusion.68
  315.2 1.1 fusion.68
  316.7 1.1 fusion.68
  318.3 1.1 fusion.68
  319.8 1.1 fusion.68
  321.5 0.3 multiply_reduce_fusion
  321.8 0.1 multiply_convert_fusion.5
  321.9 1.5 convolution_convert_fusion.1
  323.4 10.3 %psum.60 = bf16[22,512]{1,0:T(8,128)(2,1)S(1)} all-reduce(bf16[22,512]{1,0:T(8,128)(2,1)S(1)} %convolution_convert_fusion.1), channel_id=1, replica_groups=mesh['kv'=8,'tp'=4] {'tp'}, use_global_device_ids=true, to_apply=%region_14.15 | all-reduce | flops 11264 | bytes 45056 | tf_op jit(solution)/shard_map/psum | solution.py:132
  333.7 1.6 fusion.40
  335.2 3.4 fusion.39
  338.7 0.1 fusion.32
  338.8 19.8 %psum.61 = f32[22,1]{0,1:T(1,128)S(1)} all-reduce(f32[22,1]{0,1:T(1,128)S(1)} %bitcast.128), channel_id=1, replica_groups=mesh['kv'=8,'tp'=4] {'kv'}, use_global_device_ids=true, to_apply=%region_16.17 | all-reduce | flops 22 | bytes 176 | tf_op jit(solution)/shard_map/psum | solution.py:137
  358.6 52.5 %all-reduce.5.cloned.1.call-done = (f32[22,2752]{1,0:T(8,128)}, f32[22,2752]{1,0:T(8,128)}) async-done(((f32[22,2752]{1,0:T(8,128)}, f32[22,2752]{1,0:T(8,128)}), (f32[22,2752]{1,0:T(8,128)}, f32[22,2752]{1,0:T(8,128)})) %all-reduce.5.cloned.1.call-update) | async-done | bytes 484368 | tf_op jit(solution)/shard_map/psum | solution.py:142
  411.1 2.5 convolution_convert_fusion
  413.6 0.8 copy.80
  414.4 18.8 %reduce-scatter.4.cloned.1.call-done = bf16[128,22]{1,0:T(8,128)(2,1)} async-done(((bf16[512,22]{1,0:T(8,128)(2,1)}), bf16[128,22]{1,0:T(8,128)(2,1)}) %reduce-scatter.4.cloned.1.call-update) | async-done | bytes 5648
  433.2 0.8 copy.81
  434.0 0.6 add_convert_fusion
  (96 shorter events, 3.9 us)
Async XLA Ops:
  6.5 327.1 %copy-start = (bf16[512,2752]{0,1:T(8,128)(2,1)S(1)}, bf16[512,2752]{0,1:T(8,128)(2,1)}, u32[]{:S(2)}) copy-start(bf16[512,2752]{0,1:T(8,128)(2,1)} %param.27) | copy-start | bytes 8454148
  6.5 86.7 %all-reduce.7.cloned.1.call-start = ((), (), s32[]{:S(2)}) async-start(), calls=%async_computation.3 | async-start | bytes 589824 | tf_op jit(solution)/shard_map/psum | solution.py:63
  19.5 391.6 %all-reduce.5.cloned.1.call-start = ((), (), s32[]{:S(2)}) async-start(), calls=%async_computation.2 | async-start | bytes 1081344 | tf_op jit(solution)/shard_map/psum | solution.py:142
  132.8 105.6 %copy-start.1 = (f32[8,22,8]{1,2,0:T(8,128)}, f32[8,22,8]{1,2,0:T(8,128)S(1)}, u32[]{:S(2)}) copy-start(f32[8,22,8]{1,2,0:T(8,128)S(1)} %all-gather.8) | copy-start | bytes 16900
  163.5 74.9 %copy-start.2 = (f32[8,22,8]{1,2,0:T(8,128)}, f32[8,22,8]{1,2,0:T(8,128)S(1)}, u32[]{:S(2)}) copy-start(f32[8,22,8]{1,2,0:T(8,128)S(1)} %all-gather.9) | copy-start | bytes 16900
  238.4 83.1 %copy-start.5 = (f32[8]{0:T(128)S(1)}, f32[8]{0:T(128)}, u32[]{:S(2)}) copy-start(f32[8]{0:T(128)} %param.23) | copy-start | bytes 100
  238.4 83.4 %copy-start.4 = (f32[128]{0:T(128)S(1)}, f32[128]{0:T(128)}, u32[]{:S(2)}) copy-start(f32[128]{0:T(128)} %param.24) | copy-start | bytes 1540
  238.4 71.8 %slice-start = ((f32[8,22,8]{1,2,0:T(8,128)}), f32[7,22,8]{1,2,0:T(8,128)S(1)}, s32[]{:S(2)}) async-start(f32[8,22,8]{1,2,0:T(8,128)} %copy-done.1), calls=%async_computation.4 | async-start | bytes 57344 | tf_op jit(solution)/shard_map/slice | solution.py:13
  238.4 71.8 %slice-start.1 = ((f32[8,22,8]{1,2,0:T(8,128)}), f32[7,22,8]{1,2,0:T(8,128)S(1)}, s32[]{:S(2)}) async-start(f32[8,22,8]{1,2,0:T(8,128)} %copy-done.2), calls=%async_computation.5 | async-start | bytes 57344 | tf_op jit(solution)/shard_map/slice | solution.py:13
  238.4 95.2 %copy-start.3 = (f32[512]{0:T(512)S(1)}, f32[512]{0:T(512)}, u32[]{:S(2)}) copy-start(f32[512]{0:T(512)} %param.26) | copy-start | bytes 6148
  338.6 94.6 %reduce-scatter.4.cloned.1.call-start = ((), (), s32[]{:S(2)}) async-start(), calls=%async_computation.1 | async-start | bytes 163840
Sparse Core Ops, SparseCore 0:
  19.6 73.6 all-reduce.6
  338.7 72.3 all-reduce.4
  414.5 18.6 reduce-scatter.3
where the time goes:
time: 442 us; the launch traced here: 441 us
  blocking collectives  245 us (55%)
  waiting for transfers between devices  105 us (24%)
  matrix products  41.8 us (9%)
  local copies, waits for them, and re-layouts  24.2 us (5%)
  between operations  13.3 us (3%)
  other arithmetic  11.2 us (3%)
    all_gather x6, blocking collectives, combined_all(): pieces = jax.tree.map(lambda part: lax.all_gather(part, axis), value)  186 us
    psum x1, waiting for transfers between devices, per_device(): gate_sum, up_sum = lax.psum((gate_part, up_part), 'kv')  52.5 us
    psum x1, waiting for transfers between devices, per_device(): lax.psum((query_part, key_part, value_part, jnp.sum(gathered_f * gathered...  34.2 us
    psum x1, blocking collectives, per_device(): lax.psum((query_part, key_part, value_part, jnp.sum(gathered_f * gathered...  22.2 us
    psum x1, blocking collectives, per_device(): lax.psum(jnp.sum(residual_f * residual_f, axis=1, keepdims=True), 'kv')  19.8 us
    unnamed x4, waiting for transfers between devices  18.8 us
    slice x1, local copies, waits for them, and re-layouts, partial_map(): cache_keys[:, :, :, low:high]  17.3 us
    dot_general x2, matrix products, partial_map(): jnp.einsum('shd,sthd->sht', query_rows[:, :, low:high], cache_keys[:, :,...  14.7 us
  transfers between devices with their start and end apart: 3, of which 3 were waited for; matrix products, arithmetic and copies ran while one was open for 4% of the time, Pallas kernels for 0%

commit v1 on v0

--- a/solution.py
+++ b/solution.py
@@ -1,3 +1,4 @@
+import functools
 import jax
 import jax.numpy as jnp
 from jax import lax
@@ -5,6 +6,14 @@
 
 D = 4096
 epsilon = 1e-06
+
+
+def _play_leaf(slab_in, comm_axis):
+    r_now = jnp.sum(lax.all_gather(slab_in, comm_axis), 0)
+    return r_now
+
+
+arrange_sizes = functools.partial(_play_leaf, comm_axis="kv")
 
 
 def combined_all(value, axis, join):
@@ -134,7 +143,7 @@
     ).astype(jnp.float32)
     residual = (gathered_f + branch).astype(jnp.bfloat16)
     residual_f = residual.astype(jnp.float32)
-    mid_sum = lax.psum(jnp.sum(residual_f * residual_f, axis=1, keepdims=True), "kv")
+    mid_sum = arrange_sizes(jnp.sum(residual_f * residual_f, axis=1, keepdims=True))
     scale_mid = lax.rsqrt(mid_sum / D + epsilon)
     normed_mid = (residual_f * mlp_gain).astype(jnp.bfloat16)
     gate_part = jnp.dot(normed_mid, w_gate, preferred_element_type=jnp.float32)

time: 442 us -> 442 us (level)
    psum x1 -> x0, blocking collectives: 19.8 us -> none  [per_device(): lax.psum(jnp.sum(residual_f * residual_f, axis=1, keepdims=True), 'kv')]
    unnamed x0 -> x1, blocking collectives: none -> 19.6 us
where the time goes in v1:
time: 442 us; the launch traced here: 441 us
  blocking collectives  245 us (55%)
  waiting for transfers between devices  104 us (24%)
  matrix products  41.8 us (9%)
  local copies, waits for them, and re-layouts  25.1 us (6%)
  between operations  14 us (3%)
  other arithmetic  11.2 us (3%)
    all_gather x6, blocking collectives, combined_all(): pieces = jax.tree.map(lambda part: lax.all_gather(part, axis), value)  186 us
    psum x1, waiting for transfers between devices, per_device(): gate_sum, up_sum = lax.psum((gate_part, up_part), 'kv')  50.9 us
    psum x1, waiting for transfers between devices, per_device(): lax.psum((query_part, key_part, value_part, jnp.sum(gathered_f * gathered...  34.2 us
    psum x1, blocking collectives, per_device(): lax.psum((query_part, key_part, value_part, jnp.sum(gathered_f * gathered...  22.2 us
    unnamed x1, blocking collectives  19.6 us
    unnamed x4, waiting for transfers between devices  18.8 us
    slice x1, local copies, waits for them, and re-layouts, partial_map(): cache_keys[:, :, :, low:high]  17.3 us
    dot_general x2, matrix products, partial_map(): jnp.einsum('shd,sthd->sht', query_rows[:, :, low:high], cache_keys[:, :,...  14.7 us
  transfers between devices with their start and end apart: 3, of which 3 were waited for; matrix products, arithmetic and copies ran while one was open for 4% of the time, Pallas kernels for 0%

profile of v1, /device:TPU:0, one launch (start us, length us, event | category | flops | bytes accessed | tf_op | source)
XLA Modules:
  0.0 441.0 jit_solution(8839738426164571054)
XLA Ops:
  6.5 6.5 %all_gather.42 = bf16[22,512]{1,0:T(8,128)(2,1)S(1)} all-gather(bf16[22,128]{1,0:T(8,128)(2,1)} %param.16), channel_id=1, replica_groups=mesh['kv'=8,'tp'=4] {'tp'}, dimensions={1}, use_global_device_ids=true | all-gather | bytes 28160 | tf_op jit(solution)/shard_map/all_gather | solution.py:66
  13.0 2.1 fusion.35
  15.2 2.1 fusion.33
  17.3 2.1 fusion.37
  19.5 17.3 %fusion.54 = (bf16[22,256,8,64]{3,2,1,0:T(8,128)(2,1)}, bf16[22,256,8,64]{3,2,1,0:T(8,128)(2,1)}) fusion(bf16[22,256,8,128]{3,2,1,0:T(8,128)(2,1)} %param.21), kind=kLoop, calls=%fused_computation.89 | loop fusion | bytes 23068672 | tf_op jit(solution)/shard_map/slice | solution.py:90
  36.8 0.1 fusion.28
  36.9 22.2 %psum.49 = f32[22,1]{0,1:T(1,128)S(1)} all-reduce(f32[22,1]{0,1:T(1,128)S(1)} %bitcast.126), channel_id=1, replica_groups=mesh['kv'=8,'tp'=4] {'kv'}, use_global_device_ids=true, to_apply=%region_1.0 | all-reduce | flops 22 | bytes 176 | tf_op jit(solution)/shard_map/psum | solution.py:72
  59.1 34.2 %all-reduce.8.cloned.1.call-done = (f32[22,1024]{1,0:T(8,128)}, f32[22,1024]{1,0:T(8,128)}, f32[22,1024]{1,0:T(8,128)}) async-done(((f32[22,1024]{1,0:T(8,128)}, f32[22,1024]{1,0:T(8,128)}, f32[22,1024]{1,0:T(8,128)}), (f32[22,1024]{1,0:T(8,128)}, f32[22,1024]{1,0:T(8,128)}, f32[22,1024]{1,0:T(8,128)})) %all-reduce.8.cloned.1.call-update) | async-done | bytes 270352 | tf_op jit(solution)/shard_map/psum | solution.py:72
  93.3 1.1 fusion.31
  94.5 7.4 %fusion.6 = f32[22,8,1,256]{3,2,1,0:T(1,128)S(1)} fusion(bf16[22,256,8,64]{3,2,1,0:T(8,128)(2,1)} %get-tuple-element.134, bf16[22,8,64,1]{2,1,0,3:T(8,128)(2,1)S(1)} %get-tuple-element.142), kind=kOutput, calls=%fused_computation.16 | convolution fusion | flops 5767168 | bytes 5969920 | tf_op jit(solution)/shard_map/shd,sthd->sht/dot_general | solution.py:87
  101.8 0.1 fusion.21
  101.9 0.2 fusion.24
  102.2 30.6 %all-gather.9 = f32[8,22,8]{1,2,0:T(8,128)S(1)} all-gather(f32[1,22,8]{1,2,0:T(8,128)S(1)} %copy.59), channel_id=5, replica_groups=mesh['kv'=8,'tp'=4] {'kv'}, dimensions={0}, use_global_device_ids=true | all-gather | bytes 6336 | tf_op jit(solution)/shard_map/all_gather | solution.py:20
  132.9 30.6 %all-gather.10 = f32[8,22,8]{1,2,0:T(8,128)S(1)} all-gather(f32[1,22,8]{1,2,0:T(8,128)S(1)} %copy.60), channel_id=6, replica_groups=mesh['kv'=8,'tp'=4] {'kv'}, dimensions={0}, use_global_device_ids=true | all-gather | bytes 6336 | tf_op jit(solution)/shard_map/all_gather | solution.py:20
  163.5 7.4 %fusion.8 = f32[22,8,1,256]{3,2,1,0:T(1,128)S(1)} fusion(bf16[22,256,8,64]{3,2,1,0:T(8,128)(2,1)} %get-tuple-element.135, bf16[22,8,64,1]{2,1,0,3:T(8,128)(2,1)S(1)} %get-tuple-element.143), kind=kOutput, calls=%fused_computation.18 | convolution fusion | flops 5767168 | bytes 5969920 | tf_op jit(solution)/shard_map/shd,sthd->sht/dot_general | solution.py:87
  171.0 0.2 fusion.25
  171.2 30.6 %all-gather.7 = f32[8,22,8]{1,2,0:T(8,128)S(1)} all-gather(f32[1,22,8]{1,2,0:T(8,128)S(1)} %copy.57), channel_id=2, replica_groups=mesh['kv'=8,'tp'=4] {'kv'}, dimensions={0}, use_global_device_ids=true | all-gather | bytes 6336 | tf_op jit(solution)/shard_map/all_gather | solution.py:20
  201.9 30.6 %all-gather.8 = f32[8,22,8]{1,2,0:T(8,128)S(1)} all-gather(f32[1,22,8]{1,2,0:T(8,128)S(1)} %copy.58), channel_id=3, replica_groups=mesh['kv'=8,'tp'=4] {'kv'}, dimensions={0}, use_global_device_ids=true | all-gather | bytes 6336 | tf_op jit(solution)/shard_map/all_gather | solution.py:20
  232.5 5.9 %fusion.12 = f32[22,8,1,128]{3,2,1,0:T(1,128)S(1)} fusion(bf16[22,256,8,128]{3,2,1,0:T(8,128)(2,1)} %param.22, bf16[22,8,256,1]{2,1,0,3:T(8,128)(2,1)S(1)} %get-tuple-element.138), kind=kOutput, calls=%fused_computation.22 | convolution fusion | flops 11534336 | bytes 11714560 | tf_op jit(solution)/shard_map/sht,sthd->shd/dot_general | solution.py:98
  238.5 32.1 %all-gather.2 = f32[176,8,128]{2,1,0:T(8,128)S(1)} all-gather(f32[22,8,128]{2,1,0:T(8,128)S(1)} %bitcast.121), channel_id=4, replica_groups=mesh['kv'=8,'tp'=4] {'kv'}, dimensions={0}, use_global_device_ids=true | all-gather | bytes 811008 | tf_op jit(solution)/shard_map/all_gather | solution.py:20
  270.5 0.9 slice.104
  271.4 5.9 %fusion.10 = f32[22,8,1,128]{3,2,1,0:T(1,128)S(1)} fusion(bf16[22,256,8,128]{3,2,1,0:T(8,128)(2,1)} %param.22, bf16[22,8,256,1]{2,1,0,3:T(8,128)(2,1)S(1)} %get-tuple-element.136), kind=kOutput, calls=%fused_computation.20 | convolution fusion | flops 11534336 | bytes 11714560 | tf_op jit(solution)/shard_map/sht,sthd->shd/dot_general | solution.py:98
  277.3 31.7 %all-gather.5 = f32[176,8,128]{2,1,0:T(8,128)S(1)} all-gather(f32[22,8,128]{2,1,0:T(8,128)S(1)} %bitcast.122), channel_id=7, replica_groups=mesh['kv'=8,'tp'=4] {'kv'}, dimensions={0}, use_global_device_ids=true | all-gather | bytes 811008 | tf_op jit(solution)/shard_map/all_gather | solution.py:20
  309.0 0.9 slice.107
  309.9 0.2 multiply_reduce_fusion.2
  310.3 10.7 %while.20 = (s32[]{:T(128)}, f32[22,8]{0,1:T(8,128)S(1)}, f32[22,8]{0,1:T(8,128)S(1)}, f32[22,8,128]{2,1,0:T(8,128)S(1)}, f32[22,8]{0,1:T(8,128)S(1)}, /*index=5...) while((s32[]{:T(128)}, f32[22,8]{0,1:T(8,128)S(1)}, ...), condition=%wide.region_8.0_spmd, body=%wide.region_7.0_spmd.sunk | while | flops 137282 | bytes 560537 | solution.py:23
  310.6 1.1 fusion.68
  312.2 1.1 fusion.68
  313.7 1.1 fusion.68
  315.2 1.1 fusion.68
  316.7 1.1 fusion.68
  318.3 1.1 fusion.68
  319.8 1.1 fusion.68
  321.5 0.3 multiply_reduce_fusion
  321.9 1.5 convolution_convert_fusion.1
  323.4 10.3 %psum.53 = bf16[22,512]{1,0:T(8,128)(2,1)S(1)} all-reduce(bf16[22,512]{1,0:T(8,128)(2,1)S(1)} %convolution_convert_fusion.1), channel_id=1, replica_groups=mesh['kv'=8,'tp'=4] {'tp'}, use_global_device_ids=true, to_apply=%region_14.15 | all-reduce | flops 11264 | bytes 45056 | tf_op jit(solution)/shard_map/psum | solution.py:141
  333.7 1.6 fusion.40
  335.2 3.4 fusion.39
  338.7 0.6 dynamic-slice
  339.9 0.1 fusion.32
  340.0 0.2 dynamic-update-slice
  340.3 19.6 %all-reduce = f32[176]{0:T(256)S(1)} all-reduce(f32[176]{0:T(256)S(1)} %dynamic-update-slice), channel_id=8, replica_groups=mesh['kv'=8,'tp'=4] {'kv'}, use_global_device_ids=true, to_apply=%add | all-reduce | flops 176 | bytes 1408
  360.0 50.9 %all-reduce.6.cloned.1.call-done = (f32[22,2752]{1,0:T(8,128)}, f32[22,2752]{1,0:T(8,128)}) async-done(((f32[22,2752]{1,0:T(8,128)}, f32[22,2752]{1,0:T(8,128)}), (f32[22,2752]{1,0:T(8,128)}, f32[22,2752]{1,0:T(8,128)})) %all-reduce.6.cloned.1.call-update) | async-done | bytes 484368 | tf_op jit(solution)/shard_map/psum | solution.py:151
  410.9 2.5 convolution_convert_fusion
  413.4 0.8 copy.80
  414.2 18.8 %reduce-scatter.4.cloned.1.call-done = bf16[128,22]{1,0:T(8,128)(2,1)} async-done(((bf16[512,22]{1,0:T(8,128)(2,1)}), bf16[128,22]{1,0:T(8,128)(2,1)}) %reduce-scatter.4.cloned.1.call-update) | async-done | bytes 5648
  433.0 0.8 copy.81
  433.8 0.6 add_convert_fusion
  (103 shorter events, 4.2 us)
Async XLA Ops:
  6.5 327.1 %copy-start = (bf16[512,2752]{0,1:T(8,128)(2,1)S(1)}, bf16[512,2752]{0,1:T(8,128)(2,1)}, u32[]{:S(2)}) copy-start(bf16[512,2752]{0,1:T(8,128)(2,1)} %param.27) | copy-start | bytes 8454148
  6.5 86.7 %all-reduce.8.cloned.1.call-start = ((), (), s32[]{:S(2)}) async-start(), calls=%async_computation.3 | async-start | bytes 589824 | tf_op jit(solution)/shard_map/psum | solution.py:72
  19.5 391.4 %all-reduce.6.cloned.1.call-start = ((), (), s32[]{:S(2)}) async-start(), calls=%async_computation.2 | async-start | bytes 1081344 | tf_op jit(solution)/shard_map/psum | solution.py:151
  132.8 105.6 %copy-start.1 = (f32[8,22,8]{1,2,0:T(8,128)}, f32[8,22,8]{1,2,0:T(8,128)S(1)}, u32[]{:S(2)}) copy-start(f32[8,22,8]{1,2,0:T(8,128)S(1)} %all-gather.9) | copy-start | bytes 16900
  163.5 74.9 %copy-start.2 = (f32[8,22,8]{1,2,0:T(8,128)}, f32[8,22,8]{1,2,0:T(8,128)S(1)}, u32[]{:S(2)}) copy-start(f32[8,22,8]{1,2,0:T(8,128)S(1)} %all-gather.10) | copy-start | bytes 16900
  238.4 83.1 %copy-start.5 = (f32[8]{0:T(128)S(1)}, f32[8]{0:T(128)}, u32[]{:S(2)}) copy-start(f32[8]{0:T(128)} %param.23) | copy-start | bytes 100
  238.4 83.4 %copy-start.4 = (f32[128]{0:T(128)S(1)}, f32[128]{0:T(128)}, u32[]{:S(2)}) copy-start(f32[128]{0:T(128)} %param.24) | copy-start | bytes 1540
  238.4 71.8 %slice-start = ((f32[8,22,8]{1,2,0:T(8,128)}), f32[7,22,8]{1,2,0:T(8,128)S(1)}, s32[]{:S(2)}) async-start(f32[8,22,8]{1,2,0:T(8,128)} %copy-done.1), calls=%async_computation.4 | async-start | bytes 57344 | tf_op jit(solution)/shard_map/slice | solution.py:22
  238.4 71.8 %slice-start.1 = ((f32[8,22,8]{1,2,0:T(8,128)}), f32[7,22,8]{1,2,0:T(8,128)S(1)}, s32[]{:S(2)}) async-start(f32[8,22,8]{1,2,0:T(8,128)} %copy-done.2), calls=%async_computation.5 | async-start | bytes 57344 | tf_op jit(solution)/shard_map/slice | solution.py:22
  238.4 95.2 %copy-start.3 = (f32[512]{0:T(512)S(1)}, f32[512]{0:T(512)}, u32[]{:S(2)}) copy-start(f32[512]{0:T(512)} %param.26) | copy-start | bytes 6148
  271.4 67.3 %copy-start.6 = (u32[32]{0:T(128)S(1)}, u32[32]{0:T(128)}, u32[]{:S(2)}) copy-start(u32[32]{0:T(128)} %constant.45) | copy-start | bytes 388
  338.6 94.4 %reduce-scatter.4.cloned.1.call-start = ((), (), s32[]{:S(2)}) async-start(), calls=%async_computation.1 | async-start | bytes 163840
Sparse Core Ops, SparseCore 0:
  19.6 73.6 all-reduce.7
  338.7 72.1 all-reduce.5
  414.3 18.6 reduce-scatter.3
